TPU v7x, 32 devices: a whole 2x2x4 slice. The times are simulated.
32 devices in a mesh: ep: 8 (over z, x), tp: 4 (over y, core).
Axes of the slice: x: 2, y: 2, z: 4, core: 2. Of those that a mesh axis runs over, the one named last changes fastest.
Arguments:
- tokens: bfloat16 [256, 4096], P('ep'), may hold values from -6 to 6
- routes: int32 [256, 4], P('ep'), may hold values from 0 to 7, all different within a row; in each aligned block of 32 rows (0 to 31, 32 to 63, ...) at most 24 rows name the same one
- mix_weights: float32 [256, 4], P('ep'), may hold values from 0.2 to 1
- pre_gain: float32 [4096], replicated, may hold values from 0.1 to 1.9
- gate_weight: bfloat16 [8, 4096, 2048], P('ep', None, 'tp'), may hold values from -0.09375 to 0.09375
- up_weight: bfloat16 [8, 4096, 2048], P('ep', None, 'tp'), may hold values from -0.09375 to 0.09375
- down_weight: bfloat16 [8, 2048, 4096], P('ep', 'tp'), may hold values from -1 to 1
- post_gain: float32 [4096], P('tp'), may hold values from 0.1 to 1.9
Outputs:
- layer_out: bfloat16 [256, 4096], P('ep', 'tp')
Inputs may be any that keep to these rules, and one draw needn't show every extreme that they name: `routes`: within a row the 4 experts differ; among the rows of one index of ep no expert is named more than 24 times.
All inputs are finite; a program needn't handle non-finite values.
Results may differ from a plain program's by a relative error of at most 0.019.
Values may be sent and summed in bfloat16 or wider, within the bound.
A program may use at most 64 MiB of HBM per device.

v0:
```python
import jax
import jax.numpy as jnp
from jax import lax
from jax.sharding import PartitionSpec as P

epsilon = 1e-06


def on_device(
    tokens, routes, mix_weights, pre_gain, gate_weight, up_weight, down_weight, post_gain
):
    tok_rows, width = tokens.shape
    top_count = routes.shape[1]
    experts = lax.axis_size("ep")
    capacity = min(tok_rows, max(2, (3 * tok_rows * top_count + 2 * experts - 1) // (2 * experts)))
    floats = tokens.astype(jnp.float32)
    normed = (
        floats * lax.rsqrt(jnp.mean(floats * floats, axis=-1, keepdims=True) + epsilon) * pre_gain
    ).astype(jnp.bfloat16)
    chosen = routes.reshape(-1)
    onehot = (chosen[:, None] == jnp.arange(experts, dtype=jnp.int32)[None, :]).astype(jnp.int32)
    before = jnp.cumsum(onehot, axis=0) - onehot
    slot_rank = jnp.sum(before * onehot, axis=1)
    target = chosen * capacity + slot_rank
    placed = target[:, None] == jnp.arange(experts * capacity, dtype=jnp.int32)[None, :]
    by_choice = placed.reshape(tok_rows, top_count, experts * capacity)
    picked = jnp.any(by_choice, axis=1).astype(jnp.bfloat16)
    outgoing = jnp.einsum("tc,td->cd", picked, normed, preferred_element_type=jnp.float32).astype(
        jnp.bfloat16
    )
    outgoing = outgoing.reshape(experts, capacity, width)
    slice_width = width // lax.axis_size("tp")
    outgoing_part = lax.dynamic_slice_in_dim(
        outgoing, lax.axis_index("tp") * slice_width, slice_width, 2
    )
    arrived = lax.all_to_all(outgoing_part, "ep", split_axis=0, concat_axis=0, tiled=True)
    arrived = lax.all_gather(arrived, "tp", axis=2, tiled=True)
    arrived_rows = arrived.reshape(experts * capacity, width)
    gate_act = jnp.dot(arrived_rows, gate_weight[0], preferred_element_type=jnp.float32)
    up_act = jnp.dot(arrived_rows, up_weight[0], preferred_element_type=jnp.float32)
    hidden = (jax.nn.silu(gate_act) * up_act).astype(jnp.bfloat16)
    partial_value = jnp.dot(hidden, down_weight[0], preferred_element_type=jnp.float32)
    summed = lax.psum_scatter(
        partial_value.astype(jnp.bfloat16), "tp", scatter_dimension=1, tiled=True
    )
    returned = lax.all_to_all(
        summed.reshape(experts, capacity, summed.shape[1]),
        "ep",
        split_axis=0,
        concat_axis=0,
        tiled=True,
    )
    results = returned.reshape(experts * capacity, summed.shape[1]).astype(jnp.float32)
    mixing = jnp.sum(mix_weights[:, :, None] * by_choice.astype(jnp.float32), axis=1)
    mixed = jnp.dot(mixing, results, precision=lax.Precision.HIGHEST)
    squares = jnp.sum(mixed * mixed, axis=1)
    total = lax.psum(squares, "tp")
    scale = lax.rsqrt(total / width + epsilon)
    return (mixed * scale[:, None] * post_gain).astype(jnp.bfloat16)


def solution(mesh):
    in_specs = (
        P("ep", None),
        P("ep", None),
        P("ep", None),
        P(),
        P("ep", None, "tp"),
        P("ep", None, "tp"),
        P("ep", "tp", None),
        P("tp"),
    )
    out_specs = P("ep", "tp")
    return jax.shard_map(
        on_device, mesh=mesh, in_specs=in_specs, out_specs=out_specs, check_vma=False
    )
```

profile of v0, /device:TPU:0, one launch (start us, length us, event | category | flops | bytes accessed | tf_op | source)
XLA Modules:
  0.0 118.9 jit_solution(7595916630309548866)
XLA Ops:
  6.5 0.0 all-gather.2.cloned.1.call-start
  6.5 0.8 copy.21
  7.3 0.1 eq.29
  7.4 0.1 fusion.26
  7.5 0.2 reduce_window_sum.11
  7.7 0.2 select_reduce_fusion.1
  7.8 0.1 reduce_sum.39
  8.0 0.1 copy.22
  8.0 0.7 multiply_add_fusion
  8.7 0.1 fusion.25
  8.8 1.1 fusion.13
  10.0 1.6 %convolution_convert_fusion.1 = bf16[192,4096]{1,0:T(8,128)(2,1)S(1)} fusion(pred[32,192]{1,0:T(8,128)(4,1)S(1)} %fusion.25, bf16[32,4096]{1,0:T(8,128)(2,1)} %param.8, f32[4096]{0:T(1024)} %param.11, f32[32]{0:T(128)S(1)} %add_rsqrt_fusion.1), kind=kOutput, calls=%fused_computation.1 | convolution fusion | flops 51642368 | bytes 1857664 | tf_op jit(solution)/shard_map/tc,td->cd/dot_general | solution.py:28
  11.6 19.2 %all_to_all.10 = bf16[8,24,1024]{2,1,0:T(8,128)(2,1)} all-to-all(bf16[8,24,1024]{2,1,0:T(8,128)(2,1)S(1)} %constant_dynamic-slice_fusion), channel_id=1, replica_groups=mesh['ep'=8,'tp'=4] {'ep'}, dimensions={0} | all-to-all | bytes 786432 | tf_op jit(solution)/shard_map/all_to_all | solution.py:36
  30.8 0.0 all-gather.2.cloned.1.call-update
  30.9 0.0 reduce-scatter.2.cloned.1.call-start
  30.9 18.4 %all-gather.2.cloned.1.call-done = bf16[8,24,4096]{2,1,0:T(8,128)(2,1)} async-done(((bf16[8,24,1024]{2,1,0:T(8,128)(2,1)}), bf16[8,24,4096]{2,1,0:T(8,128)(2,1)}) %all-gather.2.cloned.1.call-update) | async-done | bytes 1572880 | tf_op jit(solution)/shard_map/all_gather | solution.py:37
  49.4 0.0 copy-start
  49.4 3.7 %fusion.3 = f32[192,512]{1,0:T(8,128)S(1)} fusion(bf16[192,4096]{1,0:T(8,128)(2,1)} %bitcast.26, bf16[1,4096,512]{2,1,0:T(8,128)(2,1)} %param.12), kind=kOutput, calls=%fused_computation.5 | convolution fusion | flops 805306368 | bytes 6160384 | tf_op jit(solution)/shard_map/dot_general | solution.py:39
  53.1 0.0 copy-done
  53.1 0.0 copy-start.2
  53.1 0.0 copy-start.1
  53.1 6.6 %convolution_convert_fusion = bf16[192,4096]{1,0:T(8,128)(2,1)} fusion(bf16[1,512,4096]{2,1,0:T(8,128)(2,1)} %param.14, bf16[192,4096]{1,0:T(8,128)(2,1)S(1)} %bitcast.27, bf16[1,4096,512]{2,1,0:T(8,128)(2,1)} %param.13, f32[192,512]{1,0:T(8,128)S(1)} %fusion.3), kind=kOutput, calls=%fused_computation | convolution fusion | flops 1611988992 | bytes 11927552 | tf_op jit(solution)/shard_map/dot_general | solution.py:42
  59.8 0.0 reduce-scatter.2.cloned.1.call-update
  59.8 28.1 %reduce-scatter.2.cloned.1.call-done = bf16[192,1024]{1,0:T(8,128)(2,1)} async-done(((bf16[192,4096]{1,0:T(8,128)(2,1)}), bf16[192,1024]{1,0:T(8,128)(2,1)}) %reduce-scatter.2.cloned.1.call-update) | async-done | bytes 393232 | tf_op jit(solution)/shard_map/reduce_scatter | solution.py:43
  87.9 5.5 %all-to-all-start.1 = ((bf16[8,24,1024]{2,1,0:T(8,128)(2,1)}), bf16[8,24,1024]{2,1,0:T(8,128)(2,1)S(1)}, u32[]{:S(2)}, u32[]{:S(2)}) async-start(bf16[8,24,1024]{2,1,0:T(8,128)(2,1)} %bitcast.28), calls=%async_computation.2 | async-start | bytes 786432 | tf_op jit(solution)/shard_map/all_to_all | solution.py:46
  93.4 0.0 copy-done.2
  93.4 0.1 select_reduce_fusion
  93.5 11.5 %all-to-all-done.1 = bf16[8,24,1024]{2,1,0:T(8,128)(2,1)S(1)} async-done(((bf16[8,24,1024]{2,1,0:T(8,128)(2,1)}), bf16[8,24,1024]{2,1,0:T(8,128)(2,1)S(1)}, u32[]{:S(2)}, u32[]{:S(2)}) %all-to-all-start.1) | async-done | bytes 393248 | tf_op jit(solution)/shard_map/all_to_all | solution.py:46
  105.0 0.4 multiply_reduce_fusion
  105.4 5.9 %psum.7 = f32[32]{0:T(128)S(1)} all-reduce(f32[32]{0:T(128)S(1)} %get-tuple-element.5), channel_id=1, replica_groups=mesh['ep'=8,'tp'=4] {'tp'}, use_global_device_ids=true, to_apply=%region_7.8 | all-reduce | flops 32 | bytes 256 | tf_op jit(solution)/shard_map/psum | solution.py:57
  111.3 0.0 copy-done.1
  111.3 0.7 multiply_convert_fusion
  (3 shorter events, 0.1 us)
Async XLA Ops:
  6.5 42.8 %all-gather.2.cloned.1.call-start = ((), (), s32[]{:S(2)}) async-start(), calls=%async_computation.3 | async-start | bytes 1966080 | tf_op jit(solution)/shard_map/all_gather | solution.py:37
  30.9 57.1 %reduce-scatter.2.cloned.1.call-start = ((), (), s32[]{:S(2)}) async-start(), calls=%async_computation.4 | async-start | bytes 1966080 | tf_op jit(solution)/shard_map/reduce_scatter | solution.py:43
  49.4 3.8 %copy-start = (bf16[8,24,4096]{2,1,0:T(8,128)(2,1)S(1)}, bf16[8,24,4096]{2,1,0:T(8,128)(2,1)}, u32[]{:S(2)}) copy-start(bf16[8,24,4096]{2,1,0:T(8,128)(2,1)} %all-gather.2.cloned.1.call-done) | copy-start | bytes 4718596
  53.1 40.3 %copy-start.2 = (f32[32,4]{0,1:T(4,128)S(1)}, f32[32,4]{0,1:T(4,128)}, u32[]{:S(2)}) copy-start(f32[32,4]{0,1:T(4,128)} %param.10) | copy-start | bytes 1540
  53.1 58.2 %copy-start.1 = (f32[1024]{0:T(1024)S(1)}, f32[1024]{0:T(1024)}, u32[]{:S(2)}) copy-start(f32[1024]{0:T(1024)} %param.15) | copy-start | bytes 12292
  87.9 17.1 %all-to-all-start.1 = ((bf16[8,24,1024]{2,1,0:T(8,128)(2,1)}), bf16[8,24,1024]{2,1,0:T(8,128)(2,1)S(1)}, u32[]{:S(2)}, u32[]{:S(2)}) async-start(bf16[8,24,1024]{2,1,0:T(8,128)(2,1)} %bitcast.28), calls=%async_computation.2 | async-start | bytes 786432 | tf_op jit(solution)/shard_map/all_to_all | solution.py:46
Sparse Core Ops, SparseCore 0:
  31.0 18.3 all-gather.1
  59.9 27.9 reduce-scatter.1
where the time goes:
time: 119 us
  waiting for transfers between devices  58.1 us (49%)
  blocking collectives  25.2 us (21%)
  between operations  13.5 us (11%)
  matrix products  12.3 us (10%)
  starting transfers between devices  5.53 us (5%)
  other arithmetic  3.16 us (3%)
    reduce_scatter x1, waiting for transfers between devices, on_device(): lax.psum_scatter(partial_value.astype(jnp.bfloat16), 'tp', scatter_dimens...  28.1 us
    all_to_all x1, blocking collectives, on_device(): lax.all_to_all(outgoing_part, 'ep', split_axis=0, concat_axis=0, tiled=True)  19.2 us
    all_gather x1, waiting for transfers between devices, on_device(): arrived = lax.all_gather(arrived, 'tp', axis=2, tiled=True)  18.4 us
    all_to_all x1, waiting for transfers between devices, on_device(): lax.all_to_all(summed.reshape(experts, capacity, summed.shape[1]), 'ep',...  11.5 us
    dot_general x1, matrix products, on_device(): jnp.dot(hidden, down_weight[0], preferred_element_type=jnp.float32)  6.61 us
    psum x1, blocking collectives, on_device(): total = lax.psum(squares, 'tp')  5.95 us
    all_to_all x1, starting transfers between devices, on_device(): lax.all_to_all(summed.reshape(experts, capacity, summed.shape[1]), 'ep',...  5.48 us
    dot_general x1, matrix products, on_device(): jnp.dot(arrived_rows, gate_weight[0], preferred_element_type=jnp.float32)  3.75 us
  transfers between devices with their start and end apart: 3, of which 3 were waited for; matrix products, arithmetic and copies ran while one was open for 0% of the time, Pallas kernels for 0%

commit v1 on v0

--- a/solution.py
+++ b/solution.py
@@ -1,12 +1,335 @@
+import functools
+
 import jax
 import jax.numpy as jnp
 from jax import lax
+from jax.experimental import pallas as pl
+from jax.experimental.pallas import tpu as pltpu
 from jax.sharding import PartitionSpec as P
 
 epsilon = 1e-06
-
-
-def on_device(
+CORES = 2
+MESH = pl.DeviceIdType.MESH
+VMEM_BYTES = 60 * 1024 * 1024
+MAX_COPIES = 256
+
+
+def fused_kernel(
+    S, X, NT,
+    tokens, routes, mix, pre_gain, gate_hbm, up_hbm, down_hbm, post_gain, out,
+    xg, wg, wu, wd, acc_g, acc_u, hid, wt, wr,
+    pown, dsend, drecv, ya, yar, xb, xbr, xa, xar, yb, ybr, keep_a, keep_b,
+    za, zar, zb, zbr, st,
+    wsem, ssem, gsem, mixs, mixr, dsem, yarsem, xbrsem, xarsem, ybrsem, zarsem, zbrsem, stsem,
+):
+    R = tokens.shape[0]
+    Z, Y = S // X, NT // CORES
+    Dq = xg.shape[2]
+    H = Dq // 2
+    D = tokens.shape[1]
+    K = routes.shape[1]
+    me, t = lax.axis_index("ep"), lax.axis_index("tp")
+    z, x = me // X, lax.rem(me, X)
+    y, c = t // CORES, lax.rem(t, CORES)
+    pc = 1 - c
+    f32, bf16 = jnp.float32, jnp.bfloat16
+
+    def dev(e, q):
+        return (e, q)
+
+    def quarter(yy, cc):
+        return yy * CORES + cc
+
+    zs = [lax.rem(z + d, Z) for d in range(Z)]
+    xs = [lax.rem(x + d, X) for d in range(X)]
+    ys = [lax.rem(y + d, Y) for d in range(Y)]
+    zm = [lax.rem(z - d + Z, Z) for d in range(Z)]
+    xm = [lax.rem(x - d + X, X) for d in range(X)]
+    ym = [lax.rem(y - d + Y, Y) for d in range(Y)]
+
+    loads = []
+    for i in range(NT):
+        for k, (src, dst) in enumerate(((gate_hbm, wg), (up_hbm, wu))):
+            loads.append(pltpu.make_async_copy(src.at[0, pl.ds(i * Dq, Dq)], dst.at[i], wsem.at[k, i]))
+    for i in range(NT):
+        loads.append(pltpu.make_async_copy(down_hbm.at[0, :, pl.ds(i * Dq, Dq)], wd.at[i], wsem.at[2, i]))
+    for copy in loads:
+        copy.start()
+
+    barrier = pltpu.get_barrier_semaphore()
+    for d in range(1, S):
+        pl.semaphore_signal(barrier, inc=1, device_id=dev(lax.rem(me + d, S), t), device_id_type=MESH)
+    for d in range(1, NT):
+        pl.semaphore_signal(barrier, inc=1, device_id=dev(me, lax.rem(t + d, NT)), device_id_type=MESH)
+
+    floats = tokens[...].astype(f32)
+    inv = lax.rsqrt(jnp.mean(floats * floats, axis=1, keepdims=True) + epsilon)
+    rows = pl.ds(pl.multiple_of(me * R, R), R)
+    for q in range(NT):
+        cols = slice(q * Dq, (q + 1) * Dq)
+        xg[q, rows, :] = (floats[:, cols] * inv * pre_gain[:, cols]).astype(bf16)
+
+    lane = lax.broadcasted_iota(jnp.int32, (R, 128), 1)
+    dense = jnp.zeros((R, 128), f32)
+    for k in range(K):
+        dense = dense + jnp.where(lane == routes[:, k : k + 1], mix[:, k : k + 1], 0.0)
+    flipped = jnp.transpose(jnp.concatenate([dense, jnp.zeros((128 - R, 128), f32)], axis=0))
+    for e in range(S):
+        wt[e] = flipped[e : e + 1, :]
+    wr[me] = wt[me]
+
+    pl.semaphore_wait(barrier, S - 1 + NT - 1)
+
+    sends = []
+
+    def send(src, dst, recv_sem, device):
+        copy = pltpu.make_async_remote_copy(
+            src_ref=src, dst_ref=dst, send_sem=ssem.at[len(sends)], recv_sem=recv_sem,
+            device_id=device, device_id_type=MESH,
+        )
+        copy.start()
+        sends.append(copy)
+
+    def arrived(ref, sem):
+        pltpu.make_async_remote_copy(
+            src_ref=ref, dst_ref=ref, send_sem=ssem.at[0], recv_sem=sem,
+            device_id=dev(me, t), device_id_type=MESH,
+        ).wait_recv()
+
+    def block(q, s):
+        return xg.at[q, pl.ds(pl.multiple_of(s * R, R), R)]
+
+    def send_block(q, s, device):
+        send(block(q, s), block(q, s), gsem.at[q, s], device)
+
+    def await_block(q, s):
+        arrived(block(q, s), gsem.at[q, s])
+
+    def at(d, dx):
+        return zm[d] * X + xm[dx]
+
+    for d in range(1, Z):
+        send_block(t, me, dev(zs[d] * X + x, t))
+    for dx in range(1, X):
+        send_block(t, me, dev(z * X + xs[dx], t))
+        for dy in range(1, Y):
+            send_block(quarter(ys[dy], c), me, dev(z * X + xs[dx], t))
+    for d in range(1, S):
+        e = lax.rem(me + d, S)
+        send(wt.at[e], wr.at[me], mixr.at[me], dev(e, t))
+    for d in range(1, Z):
+        s = at(d, 0)
+        await_block(t, s)
+        for dy in range(1, Y):
+            send_block(t, s, dev(me, quarter(ys[dy], c)))
+        for dx in range(1, X):
+            send_block(t, s, dev(z * X + xs[dx], t))
+        send_block(t, s, dev(me, quarter(y, pc)))
+    for dx in range(1, X):
+        for d in range(Z):
+            s = at(d, dx)
+            await_block(t, s)
+            if d > 0:
+                for dy in range(1, Y):
+                    send_block(t, s, dev(me, quarter(ys[dy], c)))
+            send_block(t, s, dev(me, quarter(y, pc)))
+            if d == 0:
+                for dy in range(1, Y):
+                    await_block(quarter(ys[dy], c), s)
+                    send_block(quarter(ys[dy], c), s, dev(me, quarter(y, pc)))
+
+    others = [at(d, dx) for dx in range(X) for d in range(Z) if d or dx]
+
+    def multiply(q, first):
+        pltpu.make_async_copy(gate_hbm.at[0, pl.ds(0, Dq)], wg.at[q], wsem.at[0, q]).wait()
+        pltpu.make_async_copy(up_hbm.at[0, pl.ds(0, Dq)], wu.at[q], wsem.at[1, q]).wait()
+        for w, acc in ((wg, acc_g), (wu, acc_u)):
+            part = jnp.dot(xg[q], w[q], preferred_element_type=f32)
+            acc[...] = part if first else acc[...] + part
+
+    multiply(t, True)
+    for s in others:
+        await_block(quarter(y, pc), s)
+    multiply(quarter(y, pc), False)
+    for dy in range(1, Y):
+        for dx in range(X):
+            for d in range(1, Z):
+                s = at(d, dx)
+                await_block(quarter(ym[dy], c), s)
+                send_block(quarter(ym[dy], c), s, dev(me, quarter(y, pc)))
+        multiply(quarter(ym[dy], c), False)
+    for dy in range(1, Y):
+        for s in others:
+            await_block(quarter(ym[dy], pc), s)
+        multiply(quarter(ym[dy], pc), False)
+
+    for d in range(1, S):
+        s = lax.rem(me + d, S)
+        arrived(wr.at[s], mixr.at[s])
+    named = jnp.concatenate([wr[s] for s in range(S)] + [jnp.zeros((128 - S, 128), f32)], axis=0)
+    columns = jnp.transpose(named)
+    weight = jnp.concatenate([columns[:R, s : s + 1] for s in range(S)], axis=0)
+    gate = acc_g[...]
+    hid[...] = (gate / (1.0 + jnp.exp(-gate)) * acc_u[...] * weight).astype(bf16)
+
+    def down(q):
+        pltpu.make_async_copy(down_hbm.at[0, :, pl.ds(0, Dq)], wd.at[q], wsem.at[2, q]).wait()
+        return jnp.dot(hid[...], wd[q], preferred_element_type=f32)
+
+    y_order = [ys[dy] for dy in range(1, Y)] + [y]
+    for yy in y_order:
+        part = down(quarter(yy, pc)).astype(bf16)
+        for h in range(2):
+            for s in range(S):
+                dsend[yy, h, s // X, s % X] = part[s * R : (s + 1) * R, h * H : (h + 1) * H]
+            send(dsend.at[yy, h], drecv.at[yy, h], dsem.at[yy, h], dev(me, quarter(y, pc)))
+    for yy in y_order:
+        part = down(quarter(yy, c))
+        for h in range(2):
+            for s in range(S):
+                pown[yy, h, s // X, s % X] = part[s * R : (s + 1) * R, h * H : (h + 1) * H]
+
+    def own(yy, h, j, xx):
+        return pown[yy, h, j, xx] + drecv[yy, h, j, xx].astype(f32)
+
+    js = [zs[d] for d in range(1, Z)] + [z]
+    for yy in y_order:
+        for h in range(2):
+            arrived(drecv.at[yy, h], dsem.at[yy, h])
+    for j in js:
+        for dy in range(1, Y):
+            for xx in range(X):
+                ya[dy, j, xx] = own(ys[dy], 0, j, xx).astype(bf16)
+            send(ya.at[dy, j], yar.at[dy, j], yarsem.at[dy, j], dev(me, quarter(ys[dy], c)))
+        for dx in range(1, X):
+            for yy in y_order:
+                xb[dx, yy, j] = own(yy, 1, j, xs[dx]).astype(bf16)
+                send(xb.at[dx, yy, j], xbr.at[dx, yy, j], xbrsem.at[dx, yy, j], dev(z * X + xs[dx], t))
+    for j in js:
+        for yy in y_order:
+            total = own(yy, 1, j, x)
+            for dx in range(1, X):
+                arrived(xbr.at[dx, yy, j], xbrsem.at[dx, yy, j])
+                total = total + xbr[dx, yy, j].astype(f32)
+            keep_b[yy, j] = total
+        for dy in range(1, Y):
+            yb[dy, j] = keep_b[ys[dy], j].astype(bf16)
+            send(yb.at[dy, j], ybr.at[dy, j], ybrsem.at[dy, j], dev(me, quarter(ys[dy], c)))
+        for dy in range(1, Y):
+            arrived(yar.at[dy, j], yarsem.at[dy, j])
+        for dx in list(range(1, X)) + [0]:
+            total = own(y, 0, j, xs[dx])
+            for dy in range(1, Y):
+                total = total + yar[dy, j, xs[dx]].astype(f32)
+            if dx == 0:
+                keep_a[j] = total
+            else:
+                xa[dx, j] = total.astype(bf16)
+                send(xa.at[dx, j], xar.at[dx, j], xarsem.at[dx, j], dev(z * X + xs[dx], t))
+    for at_d, j in enumerate(js):
+        d = (at_d + 1) % Z
+        total_a = keep_a[j]
+        for dx in range(1, X):
+            arrived(xar.at[dx, j], xarsem.at[dx, j])
+            total_a = total_a + xar[dx, j].astype(f32)
+        if d:
+            za[d] = total_a.astype(bf16)
+            send(za.at[d], zar.at[d], zarsem.at[d], dev(j * X + x, t))
+        total_b = keep_b[y, j]
+        for dy in range(1, Y):
+            arrived(ybr.at[dy, j], ybrsem.at[dy, j])
+            total_b = total_b + ybr[dy, j].astype(f32)
+        if d:
+            zb[d] = total_b.astype(bf16)
+            send(zb.at[d], zbr.at[d], zbrsem.at[d], dev(j * X + x, t))
+    for d in range(1, Z):
+        arrived(zar.at[d], zarsem.at[d])
+        total_a = total_a + zar[d].astype(f32)
+        arrived(zbr.at[d], zbrsem.at[d])
+        total_b = total_b + zbr[d].astype(f32)
+
+    squares = jnp.sum(total_a * total_a, axis=1, keepdims=True) + jnp.sum(
+        total_b * total_b, axis=1, keepdims=True
+    )
+    st[0] = jnp.broadcast_to(squares, (R, 128))
+    for d in range(1, NT):
+        send(st.at[0], st.at[d], stsem.at[d], dev(me, lax.rem(t + d, NT)))
+    for d in range(1, NT):
+        arrived(st.at[d], stsem.at[d])
+        squares = squares + st[d][:, 0:1]
+    scale = lax.rsqrt(squares / D + epsilon)
+    out[:, 0:H] = (total_a * scale * post_gain[:, 0:H]).astype(bf16)
+    out[:, H:Dq] = (total_b * scale * post_gain[:, H:Dq]).astype(bf16)
+    for copy in sends:
+        copy.wait_send()
+
+
+def fused(S, X, NT, tokens, routes, mix_weights, pre_gain, gate_weight, up_weight, down_weight, post_gain):
+    R, D = tokens.shape
+    F = gate_weight.shape[2]
+    Dq = D // NT
+    H = Dq // 2
+    Z, Y = S // X, NT // CORES
+    f32, bf16 = jnp.float32, jnp.bfloat16
+    dma, vmem = pltpu.SemaphoreType.DMA, pltpu.VMEM
+    in_vmem, anywhere = pl.BlockSpec(memory_space=pltpu.VMEM), pl.BlockSpec(memory_space=pl.ANY)
+    return pl.pallas_call(
+        functools.partial(fused_kernel, S, X, NT),
+        out_shape=jax.ShapeDtypeStruct((R, Dq), bf16),
+        in_specs=[in_vmem] * 4 + [anywhere] * 3 + [in_vmem],
+        out_specs=in_vmem,
+        scratch_shapes=[
+            vmem((NT, S * R, Dq), bf16),
+            vmem((NT, Dq, F), bf16),
+            vmem((NT, Dq, F), bf16),
+            vmem((NT, F, Dq), bf16),
+            vmem((S * R, F), f32),
+            vmem((S * R, F), f32),
+            vmem((S * R, F), bf16),
+            vmem((S, 1, 128), f32),
+            vmem((S, 1, 128), f32),
+            vmem((Y, 2, Z, X, R, H), f32),
+            vmem((Y, 2, Z, X, R, H), bf16),
+            vmem((Y, 2, Z, X, R, H), bf16),
+            vmem((Y, Z, X, R, H), bf16),
+            vmem((Y, Z, X, R, H), bf16),
+            vmem((X, Y, Z, R, H), bf16),
+            vmem((X, Y, Z, R, H), bf16),
+            vmem((X, Z, R, H), bf16),
+            vmem((X, Z, R, H), bf16),
+            vmem((Y, Z, R, H), bf16),
+            vmem((Y, Z, R, H), bf16),
+            vmem((Z, R, H), f32),
+            vmem((Y, Z, R, H), f32),
+            vmem((Z, R, H), bf16),
+            vmem((Z, R, H), bf16),
+            vmem((Z, R, H), bf16),
+            vmem((Z, R, H), bf16),
+            vmem((NT, R, 128), f32),
+            dma((3, NT)),
+            dma((MAX_COPIES,)),
+            dma((NT, S)),
+            dma((S,)),
+            dma((S,)),
+            dma((Y, 2)),
+            dma((Y, Z)),
+            dma((X, Y, Z)),
+            dma((X, Z)),
+            dma((Y, Z)),
+            dma((Z,)),
+            dma((Z,)),
+            dma((NT,)),
+        ],
+        compiler_params=pltpu.CompilerParams(
+            collective_id=0, has_side_effects=True, vmem_limit_bytes=VMEM_BYTES
+        ),
+    )(
+        tokens, routes, mix_weights, pre_gain.reshape(1, D), gate_weight, up_weight, down_weight,
+        post_gain.reshape(1, Dq),
+    )
+
+
+def routed(
     tokens, routes, mix_weights, pre_gain, gate_weight, up_weight, down_weight, post_gain
 ):
     tok_rows, width = tokens.shape
@@ -59,6 +382,13 @@
     return (mixed * scale[:, None] * post_gain).astype(jnp.bfloat16)
 
 
+def copies_of(S, X, NT):
+    Z, Y = S // X, NT // CORES
+    gather = Z - 1 + (X - 1) * Y + S - 1 + NT * S * 2 * X
+    back = 2 * Y + Z * (Y - 1 + (X - 1) * Y + Y - 1 + X - 1) + 2 * Z + NT
+    return gather + back
+
+
 def solution(mesh):
     in_specs = (
         P("ep", None),
@@ -71,6 +401,11 @@
         P("tp"),
     )
     out_specs = P("ep", "tp")
+    S, NT = mesh.shape["ep"], mesh.shape["tp"]
+    X = 2
+    on_device = routed
+    if S % X == 0 and NT % CORES == 0 and copies_of(S, X, NT) <= MAX_COPIES:
+        on_device = functools.partial(fused, S, X, NT)
     return jax.shard_map(
         on_device, mesh=mesh, in_specs=in_specs, out_specs=out_specs, check_vma=False
     )

time: 119 us -> 51.6 us (0.43)
  waiting for transfers between devices: 58.1 us -> 0 us
  Pallas kernels: 0 us -> 47.2 us
  blocking collectives: 25.2 us -> 0 us
  between operations: 13.5 us -> 0.01 us
  matrix products: 12.3 us -> 0 us
  starting transfers between devices: 5.53 us -> 0 us
  other arithmetic: 3.16 us -> 0 us
  local copies, waits for them, and re-layouts: 1.1 us -> 4.2 us
    pallas_call x0 -> x1, Pallas kernels: none -> 47.2 us  [fused(): pl.pallas_call(functools.partial(fused_kernel, S, X, NT), out_shape=jax.S...]
    reduce_scatter x1 -> x0, waiting for transfers between devices: 28.1 us -> none  [on_device(): lax.psum_scatter(partial_value.astype(jnp.bfloat16), 'tp', scatter_dimens...]
    all_to_all x1 -> x0, blocking collectives: 19.2 us -> none  [on_device(): lax.all_to_all(outgoing_part, 'ep', split_axis=0, concat_axis=0, tiled=True)]
    all_gather x1 -> x0, waiting for transfers between devices: 18.4 us -> none  [on_device(): arrived = lax.all_gather(arrived, 'tp', axis=2, tiled=True)]
    dot_general x4 -> x0, matrix products: 12.3 us -> none  [the longest x1 6.61 us: on_device(): jnp.dot(hidden, down_weight[0], preferred_element_type=jnp.float32)]
    all_to_all x1 -> x0, waiting for transfers between devices: 11.5 us -> none  [on_device(): lax.all_to_all(summed.reshape(experts, capacity, summed.shape[1]), 'ep',...]
    psum x1 -> x0, blocking collectives: 5.95 us -> none  [on_device(): total = lax.psum(squares, 'tp')]
    all_to_all x1 -> x0, starting transfers between devices: 5.48 us -> none  [on_device(): lax.all_to_all(summed.reshape(experts, capacity, summed.shape[1]), 'ep',...]
  transfers between devices with their start and end apart: 3 -> 0, of which waited for: 3 -> 0; matrix products, arithmetic and copies ran while one was open for 0% -> 0% of each run, Pallas kernels for 0% -> 0%
where the time goes in v1:
time: 51.6 us; the launch traced here: 51.4 us
  Pallas kernels  47.2 us (91%)
  local copies, waits for them, and re-layouts  4.2 us (8%)
    pallas_call x1, Pallas kernels, fused(): pl.pallas_call(functools.partial(fused_kernel, S, X, NT), out_shape=jax.S...  47.2 us
    unnamed x3, local copies, waits for them, and re-layouts  4.2 us

profile of v1, /device:TPU:0, one launch (start us, length us, event | category | flops | bytes accessed | tf_op | source)
XLA Modules:
  0.0 51.4 jit_solution(14908047913044599135)
XLA Ops:
  0.0 1.4 %copy.9.routes = s32[32,4]{1,0:T(8,128)} copy(s32[32,4]{0,1:T(4,128)} %param.9) | data formatting | bytes 1024 | tf_op args[1]
  1.4 1.4 %copy.10.mix = f32[32,4]{1,0:T(8,128)} copy(f32[32,4]{0,1:T(4,128)} %param.10) | data formatting | bytes 1024 | tf_op args[2]
  2.7 47.2 %shard_map.82 = bf16[32,1024]{1,0:T(8,128)(2,1)} custom-call(bf16[32,4096]{1,0:T(8,128)(2,1)} %tokens.1, s32[32,4]{1,0:T(8,128)} %copy.9.routes, f32[32,4]{1,0:T(8,128)} %copy.10.mix, f32[1,4096]{1,0:T(1,128)} %bitcast.2, bf16[1,4096,512]{2,1,0:T(8,128)(2,1)} %gate_hbm.1, bf16[1,4096,512]{2,1,0:T(8,128)(2,1)} %up_hbm.1, bf16[1,512,4096]{2,1,0:T(8,128)(2,1)} %down_hbm.1, ...), custom_call_target="tpu_custom_call" | custom-call | tf_op jit(solution)/shard_map/pallas_call | solution.py:276
  49.9 1.5 %copy.12 = bf16[32,1024]{1,0:T(8,128)(2,1)} copy(bf16[32,1024]{1,0:T(8,128)(2,1)} %shard_map.82) | data formatting | bytes 131072

commit v2 on v1

--- a/solution.py
+++ b/solution.py
@@ -11,7 +11,8 @@
 CORES = 2
 MESH = pl.DeviceIdType.MESH
 VMEM_BYTES = 60 * 1024 * 1024
-MAX_COPIES = 256
+MAX_COPIES = 512
+SUB = 2
 
 
 def fused_kernel(
@@ -20,14 +21,16 @@
     xg, wg, wu, wd, acc_g, acc_u, hid, wt, wr,
     pown, dsend, drecv, ya, yar, xb, xbr, xa, xar, yb, ybr, keep_a, keep_b,
     za, zar, zb, zbr, st,
-    wsem, ssem, gsem, mixs, mixr, dsem, yarsem, xbrsem, xarsem, ybrsem, zarsem, zbrsem, stsem,
+    wsem, ssem, gsem, mixr, dsem, yarsem, xbrsem, xarsem, ybrsem, zarsem, zbrsem, stsem,
 ):
     R = tokens.shape[0]
     Z, Y = S // X, NT // CORES
     Dq = xg.shape[2]
-    H = Dq // 2
+    W = 2 * SUB
+    H = Dq // W
     D = tokens.shape[1]
-    K = routes.shape[1]
+    K = routes.shape[0]
+    R2 = R // SUB
     me, t = lax.axis_index("ep"), lax.axis_index("tp")
     z, x = me // X, lax.rem(me, X)
     y, c = t // CORES, lax.rem(t, CORES)
@@ -40,10 +43,20 @@
     def quarter(yy, cc):
         return yy * CORES + cc
 
-    zs = [lax.rem(z + d, Z) for d in range(Z)]
+    def flip(v, m):
+        for b in range(m.bit_length()):
+            if m >> b & 1:
+                v = v + (1 << b) * (1 - 2 * lax.rem(v // (1 << b), 2))
+        return v
+
+    if Z & (Z - 1) == 0:
+        zs = [z] + [flip(z, m) for m in range(Z - 1, 0, -1)]
+        zm = zs
+    else:
+        zs = [lax.rem(z + d, Z) for d in range(Z)]
+        zm = [lax.rem(z - d + Z, Z) for d in range(Z)]
     xs = [lax.rem(x + d, X) for d in range(X)]
     ys = [lax.rem(y + d, Y) for d in range(Y)]
-    zm = [lax.rem(z - d + Z, Z) for d in range(Z)]
     xm = [lax.rem(x - d + X, X) for d in range(X)]
     ym = [lax.rem(y - d + Y, Y) for d in range(Y)]
 
@@ -69,13 +82,11 @@
         cols = slice(q * Dq, (q + 1) * Dq)
         xg[q, rows, :] = (floats[:, cols] * inv * pre_gain[:, cols]).astype(bf16)
 
-    lane = lax.broadcasted_iota(jnp.int32, (R, 128), 1)
-    dense = jnp.zeros((R, 128), f32)
-    for k in range(K):
-        dense = dense + jnp.where(lane == routes[:, k : k + 1], mix[:, k : k + 1], 0.0)
-    flipped = jnp.transpose(jnp.concatenate([dense, jnp.zeros((128 - R, 128), f32)], axis=0))
     for e in range(S):
-        wt[e] = flipped[e : e + 1, :]
+        dense = jnp.zeros((1, R), f32)
+        for k in range(K):
+            dense = dense + jnp.where(routes[k : k + 1, :] == e, mix[k : k + 1, :], 0.0)
+        wt[e] = jnp.concatenate([dense, jnp.zeros((1, 128 - R), f32)], axis=1)
     wr[me] = wt[me]
 
     pl.semaphore_wait(barrier, S - 1 + NT - 1)
@@ -96,47 +107,55 @@
             device_id=dev(me, t), device_id_type=MESH,
         ).wait_recv()
 
-    def block(q, s):
-        return xg.at[q, pl.ds(pl.multiple_of(s * R, R), R)]
-
-    def send_block(q, s, device):
-        send(block(q, s), block(q, s), gsem.at[q, s], device)
+    def block(q, s, i):
+        return xg.at[q, pl.ds(pl.multiple_of(s * R + i * R2, R2), R2)]
+
+    def send_block(q, s, i, device):
+        send(block(q, s, i), block(q, s, i), gsem.at[q, s, i], device)
 
     def await_block(q, s):
-        arrived(block(q, s), gsem.at[q, s])
+        for i in range(SUB):
+            arrived(block(q, s, i), gsem.at[q, s, i])
+
+    def await_part(q, s, i):
+        arrived(block(q, s, i), gsem.at[q, s, i])
 
     def at(d, dx):
         return zm[d] * X + xm[dx]
 
     for d in range(1, Z):
-        send_block(t, me, dev(zs[d] * X + x, t))
+        for i in range(SUB):
+            send_block(t, me, i, dev(zs[d] * X + x, t))
     for dx in range(1, X):
-        send_block(t, me, dev(z * X + xs[dx], t))
-        for dy in range(1, Y):
-            send_block(quarter(ys[dy], c), me, dev(z * X + xs[dx], t))
+        for i in range(SUB):
+            send_block(t, me, i, dev(z * X + xs[dx], t))
+            for dy in range(1, Y):
+                send_block(quarter(ys[dy], c), me, i, dev(z * X + xs[dx], t))
     for d in range(1, S):
         e = lax.rem(me + d, S)
         send(wt.at[e], wr.at[me], mixr.at[me], dev(e, t))
     for d in range(1, Z):
         s = at(d, 0)
-        await_block(t, s)
-        for dy in range(1, Y):
-            send_block(t, s, dev(me, quarter(ys[dy], c)))
-        for dx in range(1, X):
-            send_block(t, s, dev(z * X + xs[dx], t))
-        send_block(t, s, dev(me, quarter(y, pc)))
+        for i in range(SUB):
+            await_part(t, s, i)
+            for dx in range(1, X):
+                send_block(t, s, i, dev(z * X + xs[dx], t))
+            for dy in range(1, Y):
+                send_block(t, s, i, dev(me, quarter(ys[dy], c)))
+            send_block(t, s, i, dev(me, quarter(y, pc)))
     for dx in range(1, X):
         for d in range(Z):
             s = at(d, dx)
-            await_block(t, s)
-            if d > 0:
-                for dy in range(1, Y):
-                    send_block(t, s, dev(me, quarter(ys[dy], c)))
-            send_block(t, s, dev(me, quarter(y, pc)))
-            if d == 0:
-                for dy in range(1, Y):
-                    await_block(quarter(ys[dy], c), s)
-                    send_block(quarter(ys[dy], c), s, dev(me, quarter(y, pc)))
+            for i in range(SUB):
+                await_part(t, s, i)
+                if d > 0:
+                    for dy in range(1, Y):
+                        send_block(t, s, i, dev(me, quarter(ys[dy], c)))
+                send_block(t, s, i, dev(me, quarter(y, pc)))
+                if d == 0:
+                    for dy in range(1, Y):
+                        await_part(quarter(ys[dy], c), s, i)
+                        send_block(quarter(ys[dy], c), s, i, dev(me, quarter(y, pc)))
 
     others = [at(d, dx) for dx in range(X) for d in range(Z) if d or dx]
 
@@ -155,8 +174,9 @@
         for dx in range(X):
             for d in range(1, Z):
                 s = at(d, dx)
-                await_block(quarter(ym[dy], c), s)
-                send_block(quarter(ym[dy], c), s, dev(me, quarter(y, pc)))
+                for i in range(SUB):
+                    await_part(quarter(ym[dy], c), s, i)
+                    send_block(quarter(ym[dy], c), s, i, dev(me, quarter(y, pc)))
         multiply(quarter(ym[dy], c), False)
     for dy in range(1, Y):
         for s in others:
@@ -177,80 +197,101 @@
         return jnp.dot(hid[...], wd[q], preferred_element_type=f32)
 
     y_order = [ys[dy] for dy in range(1, Y)] + [y]
+    js = [zs[d] for d in range(1, Z)] + [z]
+    first, second = list(range(SUB)), list(range(SUB, W))
+
+    def own(yy, h, j, xx):
+        return pown[yy, h, j, xx] + drecv[yy, h, j, xx].astype(f32)
+
+    def await_core(yy, h):
+        arrived(drecv.at[yy, h], dsem.at[yy, h])
+
     for yy in y_order:
         part = down(quarter(yy, pc)).astype(bf16)
-        for h in range(2):
+        for h in second + first if yy is y else first + second:
             for s in range(S):
                 dsend[yy, h, s // X, s % X] = part[s * R : (s + 1) * R, h * H : (h + 1) * H]
             send(dsend.at[yy, h], drecv.at[yy, h], dsem.at[yy, h], dev(me, quarter(y, pc)))
-    for yy in y_order:
+    for dy in list(range(1, Y)) + [0]:
+        yy = ys[dy]
         part = down(quarter(yy, c))
-        for h in range(2):
+        for h in range(W):
             for s in range(S):
                 pown[yy, h, s // X, s % X] = part[s * R : (s + 1) * R, h * H : (h + 1) * H]
-
-    def own(yy, h, j, xx):
-        return pown[yy, h, j, xx] + drecv[yy, h, j, xx].astype(f32)
-
-    js = [zs[d] for d in range(1, Z)] + [z]
-    for yy in y_order:
-        for h in range(2):
-            arrived(drecv.at[yy, h], dsem.at[yy, h])
+        if dy:
+            for h in first:
+                await_core(yy, h)
+            for j in js:
+                for h in first:
+                    for xx in range(X):
+                        ya[dy, h, j, xx] = own(yy, h, j, xx).astype(bf16)
+                    send(ya.at[dy, h, j], yar.at[dy, h, j], yarsem.at[dy, h, j], dev(me, quarter(yy, c)))
+        for h in second:
+            await_core(yy, h)
+        for j in js:
+            for h in second:
+                for dx in range(1, X):
+                    xb[dx, yy, h - SUB, j] = own(yy, h, j, xs[dx]).astype(bf16)
+                    send(
+                        xb.at[dx, yy, h - SUB, j], xbr.at[dx, yy, h - SUB, j],
+                        xbrsem.at[dx, yy, h - SUB, j], dev(z * X + xs[dx], t),
+                    )
+    for h in first:
+        await_core(y, h)
     for j in js:
-        for dy in range(1, Y):
-            for xx in range(X):
-                ya[dy, j, xx] = own(ys[dy], 0, j, xx).astype(bf16)
-            send(ya.at[dy, j], yar.at[dy, j], yarsem.at[dy, j], dev(me, quarter(ys[dy], c)))
-        for dx in range(1, X):
+        for i in range(SUB):
             for yy in y_order:
-                xb[dx, yy, j] = own(yy, 1, j, xs[dx]).astype(bf16)
-                send(xb.at[dx, yy, j], xbr.at[dx, yy, j], xbrsem.at[dx, yy, j], dev(z * X + xs[dx], t))
-    for j in js:
-        for yy in y_order:
-            total = own(yy, 1, j, x)
-            for dx in range(1, X):
-                arrived(xbr.at[dx, yy, j], xbrsem.at[dx, yy, j])
-                total = total + xbr[dx, yy, j].astype(f32)
-            keep_b[yy, j] = total
-        for dy in range(1, Y):
-            yb[dy, j] = keep_b[ys[dy], j].astype(bf16)
-            send(yb.at[dy, j], ybr.at[dy, j], ybrsem.at[dy, j], dev(me, quarter(ys[dy], c)))
-        for dy in range(1, Y):
-            arrived(yar.at[dy, j], yarsem.at[dy, j])
-        for dx in list(range(1, X)) + [0]:
-            total = own(y, 0, j, xs[dx])
+                total = own(yy, SUB + i, j, x)
+                for dx in range(1, X):
+                    arrived(xbr.at[dx, yy, i, j], xbrsem.at[dx, yy, i, j])
+                    total = total + xbr[dx, yy, i, j].astype(f32)
+                keep_b[yy, i, j] = total
             for dy in range(1, Y):
-                total = total + yar[dy, j, xs[dx]].astype(f32)
-            if dx == 0:
-                keep_a[j] = total
-            else:
-                xa[dx, j] = total.astype(bf16)
-                send(xa.at[dx, j], xar.at[dx, j], xarsem.at[dx, j], dev(z * X + xs[dx], t))
+                yb[dy, i, j] = keep_b[ys[dy], i, j].astype(bf16)
+                send(yb.at[dy, i, j], ybr.at[dy, i, j], ybrsem.at[dy, i, j], dev(me, quarter(ys[dy], c)))
+            for dy in range(1, Y):
+                arrived(yar.at[dy, i, j], yarsem.at[dy, i, j])
+            for dx in list(range(1, X)) + [0]:
+                total = own(y, i, j, xs[dx])
+                for dy in range(1, Y):
+                    total = total + yar[dy, i, j, xs[dx]].astype(f32)
+                if dx == 0:
+                    keep_a[i, j] = total
+                else:
+                    xa[dx, i, j] = total.astype(bf16)
+                    send(xa.at[dx, i, j], xar.at[dx, i, j], xarsem.at[dx, i, j], dev(z * X + xs[dx], t))
+    mine = {}
     for at_d, j in enumerate(js):
         d = (at_d + 1) % Z
-        total_a = keep_a[j]
-        for dx in range(1, X):
-            arrived(xar.at[dx, j], xarsem.at[dx, j])
-            total_a = total_a + xar[dx, j].astype(f32)
-        if d:
-            za[d] = total_a.astype(bf16)
-            send(za.at[d], zar.at[d], zarsem.at[d], dev(j * X + x, t))
-        total_b = keep_b[y, j]
-        for dy in range(1, Y):
-            arrived(ybr.at[dy, j], ybrsem.at[dy, j])
-            total_b = total_b + ybr[dy, j].astype(f32)
-        if d:
-            zb[d] = total_b.astype(bf16)
-            send(zb.at[d], zbr.at[d], zbrsem.at[d], dev(j * X + x, t))
+        for i in range(SUB):
+            total = keep_a[i, j]
+            for dx in range(1, X):
+                arrived(xar.at[dx, i, j], xarsem.at[dx, i, j])
+                total = total + xar[dx, i, j].astype(f32)
+            if d:
+                za[d, i] = total.astype(bf16)
+                send(za.at[d, i], zar.at[d, i], zarsem.at[d, i], dev(j * X + x, t))
+            else:
+                mine[i] = total
+            total = keep_b[y, i, j]
+            for dy in range(1, Y):
+                arrived(ybr.at[dy, i, j], ybrsem.at[dy, i, j])
+                total = total + ybr[dy, i, j].astype(f32)
+            if d:
+                zb[d, i] = total.astype(bf16)
+                send(zb.at[d, i], zbr.at[d, i], zbrsem.at[d, i], dev(j * X + x, t))
+            else:
+                mine[SUB + i] = total
     for d in range(1, Z):
-        arrived(zar.at[d], zarsem.at[d])
-        total_a = total_a + zar[d].astype(f32)
-        arrived(zbr.at[d], zbrsem.at[d])
-        total_b = total_b + zbr[d].astype(f32)
-
-    squares = jnp.sum(total_a * total_a, axis=1, keepdims=True) + jnp.sum(
-        total_b * total_b, axis=1, keepdims=True
-    )
+        for i in range(SUB):
+            arrived(zar.at[d, i], zarsem.at[d, i])
+            mine[i] = mine[i] + zar[d, i].astype(f32)
+            arrived(zbr.at[d, i], zbrsem.at[d, i])
+            mine[SUB + i] = mine[SUB + i] + zbr[d, i].astype(f32)
+
+    squares = jnp.zeros((R, 1), f32)
+    for h in range(W):
+        squares = squares + jnp.sum(mine[h] * mine[h], axis=1, keepdims=True)
     st[0] = jnp.broadcast_to(squares, (R, 128))
     for d in range(1, NT):
         send(st.at[0], st.at[d], stsem.at[d], dev(me, lax.rem(t + d, NT)))
@@ -258,8 +299,9 @@
         arrived(st.at[d], stsem.at[d])
         squares = squares + st[d][:, 0:1]
     scale = lax.rsqrt(squares / D + epsilon)
-    out[:, 0:H] = (total_a * scale * post_gain[:, 0:H]).astype(bf16)
-    out[:, H:Dq] = (total_b * scale * post_gain[:, H:Dq]).astype(bf16)
+    for h in range(W):
+        cols = slice(h * H, (h + 1) * H)
+        out[:, cols] = (mine[h] * scale * post_gain[:, cols]).astype(bf16)
     for copy in sends:
         copy.wait_send()
 
@@ -268,7 +310,8 @@
     R, D = tokens.shape
     F = gate_weight.shape[2]
     Dq = D // NT
-    H = Dq // 2
+    W = 2 * SUB
+    H = Dq // W
     Z, Y = S // X, NT // CORES
     f32, bf16 = jnp.float32, jnp.bfloat16
     dma, vmem = pltpu.SemaphoreType.DMA, pltpu.VMEM
@@ -288,43 +331,42 @@
             vmem((S * R, F), bf16),
             vmem((S, 1, 128), f32),
             vmem((S, 1, 128), f32),
-            vmem((Y, 2, Z, X, R, H), f32),
-            vmem((Y, 2, Z, X, R, H), bf16),
-            vmem((Y, 2, Z, X, R, H), bf16),
-            vmem((Y, Z, X, R, H), bf16),
-            vmem((Y, Z, X, R, H), bf16),
-            vmem((X, Y, Z, R, H), bf16),
-            vmem((X, Y, Z, R, H), bf16),
-            vmem((X, Z, R, H), bf16),
-            vmem((X, Z, R, H), bf16),
-            vmem((Y, Z, R, H), bf16),
-            vmem((Y, Z, R, H), bf16),
-            vmem((Z, R, H), f32),
-            vmem((Y, Z, R, H), f32),
-            vmem((Z, R, H), bf16),
-            vmem((Z, R, H), bf16),
-            vmem((Z, R, H), bf16),
-            vmem((Z, R, H), bf16),
+            vmem((Y, W, Z, X, R, H), f32),
+            vmem((Y, W, Z, X, R, H), bf16),
+            vmem((Y, W, Z, X, R, H), bf16),
+            vmem((Y, SUB, Z, X, R, H), bf16),
+            vmem((Y, SUB, Z, X, R, H), bf16),
+            vmem((X, Y, SUB, Z, R, H), bf16),
+            vmem((X, Y, SUB, Z, R, H), bf16),
+            vmem((X, SUB, Z, R, H), bf16),
+            vmem((X, SUB, Z, R, H), bf16),
+            vmem((Y, SUB, Z, R, H), bf16),
+            vmem((Y, SUB, Z, R, H), bf16),
+            vmem((SUB, Z, R, H), f32),
+            vmem((Y, SUB, Z, R, H), f32),
+            vmem((Z, SUB, R, H), bf16),
+            vmem((Z, SUB, R, H), bf16),
+            vmem((Z, SUB, R, H), bf16),
+            vmem((Z, SUB, R, H), bf16),
             vmem((NT, R, 128), f32),
             dma((3, NT)),
-            dma((MAX_COPIES,)),
-            dma((NT, S)),
+            dma((copies_of(S, X, NT),)),
+            dma((NT, S, SUB)),
             dma((S,)),
-            dma((S,)),
-            dma((Y, 2)),
-            dma((Y, Z)),
-            dma((X, Y, Z)),
-            dma((X, Z)),
-            dma((Y, Z)),
-            dma((Z,)),
-            dma((Z,)),
+            dma((Y, W)),
+            dma((Y, SUB, Z)),
+            dma((X, Y, SUB, Z)),
+            dma((X, SUB, Z)),
+            dma((Y, SUB, Z)),
+            dma((Z, SUB)),
+            dma((Z, SUB)),
             dma((NT,)),
         ],
         compiler_params=pltpu.CompilerParams(
             collective_id=0, has_side_effects=True, vmem_limit_bytes=VMEM_BYTES
         ),
     )(
-        tokens, routes, mix_weights, pre_gain.reshape(1, D), gate_weight, up_weight, down_weight,
+        tokens, routes.T, mix_weights.T, pre_gain.reshape(1, D), gate_weight, up_weight, down_weight,
         post_gain.reshape(1, Dq),
     )
 
@@ -384,8 +426,8 @@
 
 def copies_of(S, X, NT):
     Z, Y = S // X, NT // CORES
-    gather = Z - 1 + (X - 1) * Y + S - 1 + NT * S * 2 * X
-    back = 2 * Y + Z * (Y - 1 + (X - 1) * Y + Y - 1 + X - 1) + 2 * Z + NT
+    gather = SUB * (Z - 1 + (X - 1) * Y + 3 * NT * S) + S - 1
+    back = Y * 2 * SUB + SUB * Z * (2 * (Y - 1) + (X - 1) * (Y + 1) + 2) + NT
     return gather + back
 
 

time: 51.6 us -> 49.6 us (0.961)
  local copies, waits for them, and re-layouts: 4.2 us -> 1.47 us
  Pallas kernels: 47.2 us -> 47.9 us
    unnamed x3 -> x1, local copies, waits for them, and re-layouts: 4.2 us -> 1.47 us
    pallas_call x1, Pallas kernels: 47.2 us -> 47.9 us  [fused(): pl.pallas_call(functools.partial(fused_kernel, S, X, NT), out_shape=jax.S...]
where the time goes in v2:
time: 49.6 us; the launch traced here: 49.4 us
  Pallas kernels  47.9 us (97%)
  local copies, waits for them, and re-layouts  1.47 us (3%)
    pallas_call x1, Pallas kernels, fused(): pl.pallas_call(functools.partial(fused_kernel, S, X, NT), out_shape=jax.S...  47.9 us
    unnamed x1, local copies, waits for them, and re-layouts  1.47 us

profile of v2, /device:TPU:0, one launch (start us, length us, event | category | flops | bytes accessed | tf_op | source)
XLA Modules:
  0.0 49.4 jit_solution(11287535450446475275)
XLA Ops:
  0.0 47.9 %shard_map.82 = bf16[32,1024]{1,0:T(8,128)(2,1)} custom-call(bf16[32,4096]{1,0:T(8,128)(2,1)} %tokens.1, s32[4,32]{1,0:T(4,128)} %bitcast.6, f32[4,32]{1,0:T(4,128)} %bitcast.7, f32[1,4096]{1,0:T(1,128)} %bitcast.4, bf16[1,4096,512]{2,1,0:T(8,128)(2,1)} %gate_hbm.1, bf16[1,4096,512]{2,1,0:T(8,128)(2,1)} %up_hbm.1, bf16[1,512,4096]{2,1,0:T(8,128)(2,1)} %down_hbm.1, ...), custom_call_target="tpu_custom_call" | custom-call | tf_op jit(solution)/shard_map/pallas_call | solution.py:319
  47.9 1.5 %copy.10 = bf16[32,1024]{1,0:T(8,128)(2,1)} copy(bf16[32,1024]{1,0:T(8,128)(2,1)} %shard_map.82) | data formatting | bytes 131072

commit v3 on v2

--- a/solution.py
+++ b/solution.py
@@ -52,7 +52,9 @@
     if Z & (Z - 1) == 0:
         zs = [z] + [flip(z, m) for m in range(Z - 1, 0, -1)]
         zm = zs
+        near = Z - 1
     else:
+        near = 0
         zs = [lax.rem(z + d, Z) for d in range(Z)]
         zm = [lax.rem(z - d + Z, Z) for d in range(Z)]
     xs = [lax.rem(x + d, X) for d in range(X)]
@@ -126,6 +128,9 @@
     for d in range(1, Z):
         for i in range(SUB):
             send_block(t, me, i, dev(zs[d] * X + x, t))
+            if d == near:
+                for dy in range(1, Y):
+                    send_block(quarter(ys[dy], c), me, i, dev(zs[d] * X + x, t))
     for dx in range(1, X):
         for i in range(SUB):
             send_block(t, me, i, dev(z * X + xs[dx], t))
@@ -140,19 +145,27 @@
             await_part(t, s, i)
             for dx in range(1, X):
                 send_block(t, s, i, dev(z * X + xs[dx], t))
-            for dy in range(1, Y):
-                send_block(t, s, i, dev(me, quarter(ys[dy], c)))
+            if d != near:
+                for dy in range(1, Y):
+                    send_block(t, s, i, dev(me, quarter(ys[dy], c)))
             send_block(t, s, i, dev(me, quarter(y, pc)))
+            if d == near:
+                for dy in range(1, Y):
+                    q = quarter(ys[dy], c)
+                    await_part(q, s, i)
+                    for dx in range(1, X):
+                        send_block(q, s, i, dev(z * X + xs[dx], t))
+                    send_block(q, s, i, dev(me, quarter(y, pc)))
     for dx in range(1, X):
         for d in range(Z):
             s = at(d, dx)
             for i in range(SUB):
                 await_part(t, s, i)
-                if d > 0:
+                if d not in (0, near):
                     for dy in range(1, Y):
                         send_block(t, s, i, dev(me, quarter(ys[dy], c)))
                 send_block(t, s, i, dev(me, quarter(y, pc)))
-                if d == 0:
+                if d in (0, near):
                     for dy in range(1, Y):
                         await_part(quarter(ys[dy], c), s, i)
                         send_block(quarter(ys[dy], c), s, i, dev(me, quarter(y, pc)))
@@ -173,6 +186,8 @@
     for dy in range(1, Y):
         for dx in range(X):
             for d in range(1, Z):
+                if d == near:
+                    continue
                 s = at(d, dx)
                 for i in range(SUB):
                     await_part(quarter(ym[dy], c), s, i)
@@ -206,14 +221,13 @@
     def await_core(yy, h):
         arrived(drecv.at[yy, h], dsem.at[yy, h])
 
-    for yy in y_order:
+    for dy in list(range(1, Y)) + [0]:
+        yy = ys[dy]
         part = down(quarter(yy, pc)).astype(bf16)
-        for h in second + first if yy is y else first + second:
+        for h in first + second if dy else second + first:
             for s in range(S):
                 dsend[yy, h, s // X, s % X] = part[s * R : (s + 1) * R, h * H : (h + 1) * H]
             send(dsend.at[yy, h], drecv.at[yy, h], dsem.at[yy, h], dev(me, quarter(y, pc)))
-    for dy in list(range(1, Y)) + [0]:
-        yy = ys[dy]
         part = down(quarter(yy, c))
         for h in range(W):
             for s in range(S):
@@ -426,7 +440,7 @@
 
 def copies_of(S, X, NT):
     Z, Y = S // X, NT // CORES
-    gather = SUB * (Z - 1 + (X - 1) * Y + 3 * NT * S) + S - 1
+    gather = SUB * ((Z - 1 + X - 1) * Y + 3 * NT * S) + S - 1
     back = Y * 2 * SUB + SUB * Z * (2 * (Y - 1) + (X - 1) * (Y + 1) + 2) + NT
     return gather + back
 

time: 49.6 us -> 49.2 us (level)
  no operation moved by 1% of the time
where the time goes in v3:
time: 49.2 us; the launch traced here: 49.1 us
  Pallas kernels  47.6 us (97%)
  local copies, waits for them, and re-layouts  1.47 us (3%)
    pallas_call x1, Pallas kernels, fused(): pl.pallas_call(functools.partial(fused_kernel, S, X, NT), out_shape=jax.S...  47.6 us
    unnamed x1, local copies, waits for them, and re-layouts  1.47 us

profile of v3, /device:TPU:0, one launch (start us, length us, event | category | flops | bytes accessed | tf_op | source)
XLA Modules:
  0.0 49.1 jit_solution(6165613165569177836)
XLA Ops:
  0.0 47.6 %shard_map.82 = bf16[32,1024]{1,0:T(8,128)(2,1)} custom-call(bf16[32,4096]{1,0:T(8,128)(2,1)} %tokens.1, s32[4,32]{1,0:T(4,128)} %bitcast.6, f32[4,32]{1,0:T(4,128)} %bitcast.7, f32[1,4096]{1,0:T(1,128)} %bitcast.4, bf16[1,4096,512]{2,1,0:T(8,128)(2,1)} %gate_hbm.1, bf16[1,4096,512]{2,1,0:T(8,128)(2,1)} %up_hbm.1, bf16[1,512,4096]{2,1,0:T(8,128)(2,1)} %down_hbm.1, ...), custom_call_target="tpu_custom_call" | custom-call | tf_op jit(solution)/shard_map/pallas_call | solution.py:333
  47.6 1.5 %copy.10 = bf16[32,1024]{1,0:T(8,128)(2,1)} copy(bf16[32,1024]{1,0:T(8,128)(2,1)} %shard_map.82) | data formatting | bytes 131072

commit v4 on v3

--- a/solution.py
+++ b/solution.py
@@ -12,7 +12,7 @@
 MESH = pl.DeviceIdType.MESH
 VMEM_BYTES = 60 * 1024 * 1024
 MAX_COPIES = 512
-SUB = 2
+SUB = 1
 
 
 def fused_kernel(
@@ -50,9 +50,9 @@
         return v
 
     if Z & (Z - 1) == 0:
-        zs = [z] + [flip(z, m) for m in range(Z - 1, 0, -1)]
+        zs = [z] + [flip(z, m) for m in range(1, Z)]
         zm = zs
-        near = Z - 1
+        near = 1
     else:
         near = 0
         zs = [lax.rem(z + d, Z) for d in range(Z)]

time: 49.2 us -> 47.9 us (0.974)
  Pallas kernels: 47.6 us -> 46.3 us
    pallas_call x1, Pallas kernels: 47.6 us -> 46.3 us  [fused(): pl.pallas_call(functools.partial(fused_kernel, S, X, NT), out_shape=jax.S...]
where the time goes in v4:
time: 47.9 us; the launch traced here: 47.8 us
  Pallas kernels  46.3 us (97%)
  local copies, waits for them, and re-layouts  1.47 us (3%)
    pallas_call x1, Pallas kernels, fused(): pl.pallas_call(functools.partial(fused_kernel, S, X, NT), out_shape=jax.S...  46.3 us
    unnamed x1, local copies, waits for them, and re-layouts  1.47 us

profile of v4, /device:TPU:0, one launch (start us, length us, event | category | flops | bytes accessed | tf_op | source)
XLA Modules:
  0.0 47.8 jit_solution(13463269120194612800)
XLA Ops:
  0.0 46.3 %shard_map.82 = bf16[32,1024]{1,0:T(8,128)(2,1)} custom-call(bf16[32,4096]{1,0:T(8,128)(2,1)} %tokens.1, s32[4,32]{1,0:T(4,128)} %bitcast.6, f32[4,32]{1,0:T(4,128)} %bitcast.7, f32[1,4096]{1,0:T(1,128)} %bitcast.4, bf16[1,4096,512]{2,1,0:T(8,128)(2,1)} %gate_hbm.1, bf16[1,4096,512]{2,1,0:T(8,128)(2,1)} %up_hbm.1, bf16[1,512,4096]{2,1,0:T(8,128)(2,1)} %down_hbm.1, ...), custom_call_target="tpu_custom_call" | custom-call | tf_op jit(solution)/shard_map/pallas_call | solution.py:333
  46.3 1.5 %copy.10 = bf16[32,1024]{1,0:T(8,128)(2,1)} copy(bf16[32,1024]{1,0:T(8,128)(2,1)} %shard_map.82) | data formatting | bytes 131072
